TPU v7x, 32 devices: a whole 2x2x4 slice. The times are simulated.
32 devices in a mesh: sp: 16 (over z, y, x), tp: 2 (over core).
Axes of the slice: x: 2, y: 2, z: 4, core: 2. Of those that a mesh axis runs over, the one named last changes fastest.
Arguments:
- residual: bfloat16 [2048, 2048], P(('sp', 'tp')), may hold values from -6 to 6
- query_wide: bfloat16 [2048, 1024], P('sp', 'tp'), may hold values from -6 to 6
- key_wide: bfloat16 [2048, 1024], P('sp', 'tp'), may hold values from -6 to 6
- value_wide: bfloat16 [2048, 2048], P('sp', 'tp'), may hold values from -6 to 6
- outgate_wide: bfloat16 [2048, 2048], P('sp', 'tp'), may hold values from -6 to 6
- gating_wide: float32 [3, 8, 2048], P(None, 'tp', 'sp'), may hold values from -4 to 240, as said below
- gain_wide: bfloat16 [2048], P('tp'), may hold values from 0.099609375 to 1.8984375
- readout_wide: bfloat16 [2048, 2048], P('tp'), may hold values from -0.109375 to 0.109375
- query_narrow: bfloat16 [2048, 512], P('sp', 'tp'), may hold values from -6 to 6
- key_narrow: bfloat16 [2048, 512], P('sp', 'tp'), may hold values from -6 to 6
- value_narrow: bfloat16 [2048, 1024], P('sp', 'tp'), may hold values from -6 to 6
- outgate_narrow: bfloat16 [2048, 1024], P('sp', 'tp'), may hold values from -6 to 6
- gating_narrow: float32 [3, 8, 2048], P(None, 'tp', 'sp'), may hold values from -4 to 240, as said below
- gain_narrow: bfloat16 [1024], P('tp'), may hold values from 0.099609375 to 1.8984375
- readout_narrow: bfloat16 [1024, 2048], P('tp'), may hold values from -0.109375 to 0.109375
- norm_gain: bfloat16 [2048], replicated, may hold values from 0.099609375 to 1.8984375
- gate_weight: bfloat16 [2048, 5632], P('sp', 'tp'), may hold values from -0.125 to 0.125
- up_weight: bfloat16 [2048, 5632], P('sp', 'tp'), may hold values from -0.125 to 0.125
- down_weight: bfloat16 [5632, 2048], P('tp', 'sp'), may hold values from -0.078125 to 0.078125
Outputs:
- mixed_out: bfloat16 [2048, 2048], P(('sp', 'tp'))
Inputs may be any that keep to these rules, and one draw needn't show every extreme that they name: `gating_wide`: row 0 holds input gate pre-activations, row 1 forget gate pre-activations, row 2 an added log-decay that is zero or negative. `gating_narrow`: row 0 holds input gate pre-activations, row 1 forget gate pre-activations, row 2 an added log-decay that is zero or negative.
All inputs are finite; a program needn't handle non-finite values.
Results may differ from a plain program's by a relative error of at most 0.017.
Values may be sent and summed in bfloat16 or wider, within the bound.
A program may use at most 128 MiB of HBM per device.

v0:
```python
import jax
import jax.numpy as jnp
from jax import lax
from jax.sharding import PartitionSpec as P

DK_A = 128
DK_B = 64
BLOCK = 64


def entering(value, axis, combine, identity):
    length, here = (lax.axis_size(axis), lax.axis_index(axis))
    everything = jax.tree.map(lambda part: lax.all_gather(part, axis), value)
    start = jax.tree.map(
        lambda part, zero: jnp.broadcast_to(jnp.asarray(zero, part.dtype), part.shape),
        value,
        identity,
    )

    def step(k, before):
        reached = k < here
        new = combine(before, jax.tree.map(lambda part: part[k], everything))
        return jax.tree.map(lambda a, b: jnp.where(reached, a, b), new, before)

    return lax.fori_loop(0, length, step, start)


def local_pass(query, key_rows, value, gating, key_size):
    rows = query.shape[0]
    attention_tally = gating.shape[1]
    value_size = value.shape[1] // attention_tally
    nblocks = rows // BLOCK
    scale = key_size ** (-0.5)
    queries = query.reshape(nblocks, BLOCK, attention_tally, key_size)
    keys_all = key_rows.reshape(nblocks, BLOCK, attention_tally, key_size)
    values_all = value.reshape(nblocks, BLOCK, attention_tally, value_size)
    incoming_matrix = jnp.moveaxis(gating[0].reshape(attention_tally, nblocks, BLOCK), 1, 0)
    forget_log = jax.nn.log_sigmoid(gating[1]) + gating[2]
    forgets = jnp.moveaxis(forget_log.reshape(attention_tally, nblocks, BLOCK), 1, 0)
    causal = jnp.tril(jnp.ones((BLOCK, BLOCK), dtype=bool))

    def advance(carry, blocks):
        memory, level = carry
        q_block, k_block, v_block, in_block, f_block = blocks
        cumul = jnp.cumsum(f_block, axis=-1)
        logits = cumul[:, :, None] - cumul[:, None, :] + in_block[:, None, :]
        logits = jnp.where(causal, logits, -jnp.inf)
        carried = cumul + level[:, None]
        stab = jnp.maximum(carried, jnp.max(logits, axis=-1))
        weights = jnp.exp(logits - stab[:, :, None])
        scores = (
            jnp.einsum("thd,shd->hts", q_block, k_block, preferred_element_type=jnp.float32) * scale
        )
        weighted = (scores * weights).astype(jnp.bfloat16)
        within = jnp.einsum("hts,shv->thv", weighted, v_block, preferred_element_type=jnp.float32)
        earlier = jnp.einsum(
            "thd,hdv->thv", q_block.astype(jnp.float32), memory, precision=lax.Precision.HIGHEST
        )
        earlier = earlier * jnp.exp(carried - stab).T[:, :, None]
        last = cumul[:, -1]
        tail = last[:, None] - cumul + in_block
        level_new = jnp.maximum(last + level, jnp.max(tail, axis=-1))
        tail_weights = jnp.exp(tail - level_new[:, None]) * scale
        scaled_keys = (k_block * tail_weights.T[:, :, None]).astype(jnp.bfloat16)
        memory_new = jnp.exp(last + level - level_new)[:, None, None] * memory
        memory_new = memory_new + jnp.einsum(
            "shd,shv->hdv", scaled_keys, v_block, preferred_element_type=jnp.float32
        )
        return ((memory_new, level_new), (within + earlier, stab))

    init = (
        jnp.zeros((attention_tally, key_size, value_size), jnp.float32),
        jnp.full((attention_tally,), -1e30, jnp.float32),
    )
    (memory_end, level_end), (raw, stabs) = lax.scan(
        advance, init, (queries, keys_all, values_all, incoming_matrix, forgets)
    )
    raw = raw.reshape(rows, attention_tally, value_size)
    stabs = jnp.moveaxis(stabs, 0, 1).reshape(attention_tally, rows)
    running = jnp.cumsum(forget_log, axis=1)
    return (raw, stabs, running, memory_end, level_end, running[:, -1])


def merge_states(earlier, later):
    merged = []
    for group in range(2):
        memory_e, level_e, total_e = earlier[3 * group : 3 * group + 3]
        memory_l, level_l, total_l = later[3 * group : 3 * group + 3]
        level = jnp.maximum(level_e + total_l, level_l)
        memory = (
            jnp.exp(level_e + total_l - level)[:, None, None] * memory_e
            + jnp.exp(level_l - level)[:, None, None] * memory_l
        )
        merged.extend([memory, level, total_e + total_l])
    return tuple(merged)


def finish_group(query, raw, stabs, running, memory_in, level_in, gain, outgate, key_size):
    rows, attention_tally, value_size = raw.shape
    shifted = running + level_in[:, None]
    stab = jnp.maximum(stabs, shifted)
    own = raw * jnp.exp(stabs - stab).T[:, :, None]
    queries = query.reshape(rows, attention_tally, key_size).astype(jnp.float32)
    incoming = jnp.einsum("thd,hdv->thv", queries, memory_in, precision=lax.Precision.HIGHEST)
    total = own + incoming * jnp.exp(shifted - stab).T[:, :, None]
    normal_raw = total * lax.rsqrt(jnp.mean(total * total, axis=-1, keepdims=True) + 1e-06)
    flat = normal_raw.reshape(rows, attention_tally * value_size)
    flat = flat * gain.astype(jnp.float32) * jax.nn.sigmoid(outgate.astype(jnp.float32))
    return flat.astype(jnp.bfloat16)


def norm_rows(middle_f, norm_gain):
    normed = middle_f * lax.rsqrt(jnp.mean(middle_f * middle_f, axis=-1, keepdims=True) + 1e-06)
    return (normed * norm_gain.astype(jnp.float32)).astype(jnp.bfloat16)


def body(
    residual,
    query_wide,
    key_wide,
    value_wide,
    outgate_wide,
    gating_wide,
    gain_wide,
    readout_wide,
    query_narrow,
    key_narrow,
    value_narrow,
    outgate_narrow,
    gating_narrow,
    gain_narrow,
    readout_narrow,
    norm_gain,
    gate_weight,
    up_weight,
    down_weight,
):
    raw_w, stabs_w, running_w, memory_w, level_w, total_w = local_pass(
        query_wide, key_wide, value_wide, gating_wide, DK_A
    )
    raw_n, stabs_n, running_n, memory_n, level_n, total_n = local_pass(
        query_narrow, key_narrow, value_narrow, gating_narrow, DK_B
    )
    carried = entering(
        (memory_w, level_w, total_w, memory_n, level_n, total_n),
        "sp",
        merge_states,
        (
            jnp.zeros_like(memory_w),
            jnp.full_like(level_w, -1e30),
            jnp.zeros_like(total_w),
            jnp.zeros_like(memory_n),
            jnp.full_like(level_n, -1e30),
            jnp.zeros_like(total_n),
        ),
    )
    gated_w = finish_group(
        query_wide, raw_w, stabs_w, running_w, carried[0], carried[1], gain_wide, outgate_wide, DK_A
    )
    gated_n = finish_group(
        query_narrow,
        raw_n,
        stabs_n,
        running_n,
        carried[3],
        carried[4],
        gain_narrow,
        outgate_narrow,
        DK_B,
    )
    mixed = lax.psum_scatter(
        (
            jnp.dot(gated_w, readout_wide, preferred_element_type=jnp.float32)
            + jnp.dot(gated_n, readout_narrow, preferred_element_type=jnp.float32)
        ).astype(jnp.bfloat16),
        "tp",
        scatter_dimension=0,
        tiled=True,
    ).astype(jnp.float32)
    middle_f = (residual.astype(jnp.float32) + mixed).astype(jnp.bfloat16).astype(jnp.float32)
    normed = norm_rows(middle_f, norm_gain)
    all_rows = lax.all_gather(normed, "tp", axis=0, tiled=True)
    gate = jnp.dot(
        all_rows,
        lax.all_gather(gate_weight, "sp", axis=0, tiled=True),
        preferred_element_type=jnp.float32,
    )
    upper = jnp.dot(
        all_rows,
        lax.all_gather(up_weight, "sp", axis=0, tiled=True),
        preferred_element_type=jnp.float32,
    )
    hidden = (jax.nn.silu(gate) * upper).astype(jnp.bfloat16)
    terms = jnp.dot(
        hidden,
        lax.all_gather(down_weight, "sp", axis=1, tiled=True),
        preferred_element_type=jnp.float32,
    )
    back = lax.psum_scatter(
        terms.astype(jnp.bfloat16), "tp", scatter_dimension=0, tiled=True
    ).astype(jnp.float32)
    return (middle_f + back).astype(jnp.bfloat16)


def solution(mesh):
    in_specs = (
        P(("sp", "tp"), None),
        P("sp", "tp"),
        P("sp", "tp"),
        P("sp", "tp"),
        P("sp", "tp"),
        P(None, "tp", "sp"),
        P("tp"),
        P("tp", None),
        P("sp", "tp"),
        P("sp", "tp"),
        P("sp", "tp"),
        P("sp", "tp"),
        P(None, "tp", "sp"),
        P("tp"),
        P("tp", None),
        P(),
        P("sp", "tp"),
        P("sp", "tp"),
        P("tp", "sp"),
    )
    out_specs = P(("sp", "tp"), None)
    return jax.shard_map(body, mesh=mesh, in_specs=in_specs, out_specs=out_specs, check_vma=False)
```

profile of v0, /device:TPU:0, one launch (start us, length us, event | category | flops | bytes accessed | tf_op | source)
XLA Modules:
  0.0 764.9 jit_solution(13011065428079746588)
XLA Ops:
  10.6 5.3 while.55
  19.7 19.3 %while.54 = (s32[]{:T(128)}, f32[4,128,256]{2,1,0:T(8,128)S(1)}, f32[4]{0:T(128)}, f32[2,64,4,256]{3,1,0,2:T(8,128)}, f32[2,4,64]{2,1,0:T(4,128)}, /*index=5*/f3...) while((s32[]{:T(128)}, f32[4,128,256]{2,1,0:T(8,128)S(1)}, ...), condition=%wide.region_4.5_spmd.clone, body=%wide.region_0.4_spmd.clone.sunk | while | flops 130980880 | bytes 3455009 | solution.py:75
  21.8 1.3 add_maximum_fusion.4
  27.8 1.3 fusion.153
  31.8 1.3 add_maximum_fusion.4
  37.8 1.2 fusion.153
  40.0 1.6 copy.70
  41.5 1.3 dynamic-slice
  48.0 44.1 %all-reduce.4 = (f32[64]{0:T(128)S(1)}, f32[64]{0:T(128)S(1)}, f32[64]{0:T(128)S(1)}, f32[64]{0:T(128)S(1)}) all-reduce(f32[64]{0:T(128)S(1)} %dynamic-update-slice, f32[64]{0:T(128)S(1)} %dynamic-update-slice.1, f32[64]{0:T(128)S(1)} %dynamic-update-slice.2, f32[64]{0:T(128)S(1)} %dynamic-update-slice.3), channel_id=2, replica_groups=mesh['sp'=16,'tp'=2] {'sp'}, use_global_device_ids=true, to_apply=%add | all-reduce | flops 256 | bytes 2048
  97.4 1.2 copy.63
  98.7 1.3 convert_element_type.74
  99.9 1.3 convert_element_type.77
  101.2 93.0 %all-gather.18.cloned.1.call-done = f32[64,128,256]{2,1,0:T(8,128)} async-done(((f32[4,128,256]{2,1,0:T(8,128)}), f32[64,128,256]{2,1,0:T(8,128)}) %all-gather.18.cloned.1.call-update) | async-done | bytes 8388624 | tf_op jit(solution)/shard_map/all_gather | solution.py:13
  194.2 56.7 %while.56 = (s32[]{:T(128)}, f32[4,128,256]{2,1,0:T(8,128)S(1)}, f32[4]{0:T(128)}, f32[4,64,128]{2,1,0:T(8,128)S(1)}, f32[4]{0:T(128)}, /*index=5*/s32[]{:T(128)...) while((s32[]{:T(128)}, f32[4,128,256]{2,1,0:T(8,128)S(1)}, ...), condition=%wide.region_13.14_spmd.clone, body=%wide.region_12.13_spmd.clone.sunk | while | flops 819260 | bytes 1966609 | solution.py:25
  194.2 1.3 broadcast_select_fusion.9
  195.5 1.2 fusion.162
  197.8 1.3 broadcast_select_fusion.9
  199.1 1.2 fusion.162
  201.3 1.3 broadcast_select_fusion.9
  202.6 1.2 fusion.162
  204.9 1.3 broadcast_select_fusion.9
  206.2 1.2 fusion.162
  208.4 1.3 broadcast_select_fusion.9
  209.7 1.2 fusion.162
  212.0 1.3 broadcast_select_fusion.9
  215.5 1.3 broadcast_select_fusion.9
  219.1 1.3 broadcast_select_fusion.9
  222.6 1.3 broadcast_select_fusion.9
  226.2 1.3 broadcast_select_fusion.9
  229.7 1.3 broadcast_select_fusion.9
  233.2 1.3 broadcast_select_fusion.9
  236.8 1.3 broadcast_select_fusion.9
  240.3 1.3 broadcast_select_fusion.9
  243.9 1.3 broadcast_select_fusion.9
  247.4 1.3 broadcast_select_fusion.9
  251.8 1.3 multiply_reduce_fusion.1
  254.8 1.5 multiply_reduce_fusion
  256.7 3.0 fusion.76
  259.8 1.3 fusion.67
  262.9 4.4 reduce-scatter.3.cloned.1.call-done
  269.6 2.4 all_gather.52
  272.0 140.6 %all-gather.12.cloned.1.call-done = bf16[2048,2816]{1,0:T(8,128)(2,1)} async-done(((bf16[128,2816]{1,0:T(8,128)(2,1)}), bf16[2048,2816]{1,0:T(8,128)(2,1)}) %all-gather.12.cloned.1.call-update) | async-done | bytes 11534352 | tf_op jit(solution)/shard_map/all_gather | solution.py:185
  412.5 7.1 fusion.118
  419.6 135.2 %all-gather.14.cloned.1.call-done = bf16[2048,2816]{1,0:T(8,128)(2,1)} async-done(((bf16[128,2816]{1,0:T(8,128)(2,1)}), bf16[2048,2816]{1,0:T(8,128)(2,1)}) %all-gather.14.cloned.1.call-update) | async-done | bytes 11534352 | tf_op jit(solution)/shard_map/all_gather | solution.py:190
  554.8 182.8 %all-gather.16.cloned.1.call-done = bf16[2816,2048]{1,0:T(8,128)(2,1)} async-done(((bf16[2816,128]{1,0:T(8,128)(2,1)}), bf16[2816,2048]{1,0:T(8,128)(2,1)}) %all-gather.16.cloned.1.call-update) | async-done | bytes 11534352 | tf_op jit(solution)/shard_map/all_gather | solution.py:196
  737.6 12.4 %convolution_convert_fusion = bf16[128,2048]{1,0:T(8,128)(2,1)} fusion(bf16[2816,2048]{1,0:T(8,128)(2,1)} %all-gather.16.cloned.1.call-done, bf16[128,2048]{1,0:T(8,128)(2,1)S(1)} %all_gather.52, bf16[2048,2816]{1,0:T(8,128)(2,1)} %all-gather.14.cloned.1.call-done, f32[128,2816]{1,0:T(8,128)} %fusion.118), kind=kOutput, calls=%fused_computation.130 | convolution fusion | flops 2955214848 | bytes 25559040 | tf_op jit(solution)/shard_map/dot_general | solution.py:194
  750.0 6.3 reduce-scatter.5.cloned.1.call-done
  756.3 1.7 fusion.75
  (240 shorter events, 74.2 us)
Async XLA Ops:
  6.5 253.2 %copy-start = (bf16[512,2048]{1,0:T(8,128)(2,1)S(1)}, bf16[512,2048]{1,0:T(8,128)(2,1)}, u32[]{:S(2)}) copy-start(bf16[512,2048]{1,0:T(8,128)(2,1)} %param.39) | copy-start | bytes 6291460
  6.5 94.7 %all-gather.20.cloned.1.call-start = ((), (), s32[]{:S(2)}) async-start(), calls=%async_computation.8 | async-start | bytes 2228224 | tf_op jit(solution)/shard_map/all_gather | solution.py:13
  10.6 6.1 copy-start.15
  10.6 7.0 copy-start.8
  10.6 7.1 copy-start.11
  10.6 7.2 copy-start.7
  15.9 0.6 copy-start.3
  15.9 1.6 copy-start.12
  15.9 1.6 copy-start.16
  16.6 177.6 %all-gather.18.cloned.1.call-start = ((), (), s32[]{:S(2)}) async-start(), calls=%async_computation.7 | async-start | bytes 8912896 | tf_op jit(solution)/shard_map/all_gather | solution.py:13
  20.4 2.7 copy-start.6
  21.0 2.1 copy-start.9
  29.8 3.3 copy-start.6
  31.0 2.1 copy-start.9
  39.0 0.8 copy-start.2
  39.9 227.5 %reduce-scatter.3.cloned.1.call-start = ((), (), s32[]{:S(2)}) async-start(), calls=%async_computation.2 | async-start | bytes 786432 | tf_op jit(solution)/shard_map/reduce_scatter | solution.py:171
  46.1 51.3 %copy-start.13 = (f32[4,128]{1,0:T(4,128)}, f32[4,128]{1,0:T(4,128)S(1)}, u32[]{:S(2)}) copy-start(f32[4,128]{1,0:T(4,128)S(1)} %reduce_window_sum.38) | copy-start | bytes 6148
  47.5 49.9 %copy-start.14 = (f32[4,128]{1,0:T(4,128)}, f32[4,128]{1,0:T(4,128)S(1)}, u32[]{:S(2)}) copy-start(f32[4,128]{1,0:T(4,128)S(1)} %reduce_window_sum.39) | copy-start | bytes 6148
  251.0 5.7 copy-start.19
  256.4 3.3 copy-start.10
  256.4 3.3 copy-start.17
  259.7 3.2 copy-start.18
  259.7 7.6 copy-start.4
  261.1 151.4 %all-gather.12.cloned.1.call-start = ((), (), s32[]{:S(2)}) async-start(), calls=%async_computation.3 | async-start | bytes 12255232 | tf_op jit(solution)/shard_map/all_gather | solution.py:185
  261.7 293.1 %all-gather.14.cloned.1.call-start = ((), (), s32[]{:S(2)}) async-start(), calls=%async_computation.4 | async-start | bytes 12255232 | tf_op jit(solution)/shard_map/all_gather | solution.py:190
  262.3 475.3 %all-gather.16.cloned.1.call-start = ((), (), s32[]{:S(2)}) async-start(), calls=%async_computation.5 | async-start | bytes 12255232 | tf_op jit(solution)/shard_map/all_gather | solution.py:196
  262.8 493.5 %reduce-scatter.5.cloned.1.call-start = ((), (), s32[]{:S(2)}) async-start(), calls=%async_computation.6 | async-start | bytes 786432 | tf_op jit(solution)/shard_map/reduce_scatter | solution.py:199
  419.6 336.7 %copy-start.5 = (bf16[64,2048]{1,0:T(8,128)(2,1)S(1)}, bf16[64,2048]{1,0:T(8,128)(2,1)}, u32[]{:S(2)}) copy-start(bf16[64,2048]{1,0:T(8,128)(2,1)} %reduce-scatter.3.cloned.1.call-done) | copy-start | bytes 786436
  737.6 20.5 %copy-start.1 = (bf16[512,2048]{1,0:T(8,128)(2,1)S(1)}, bf16[512,2048]{1,0:T(8,128)(2,1)}, u32[]{:S(2)}) copy-start(bf16[512,2048]{1,0:T(8,128)(2,1)} %param.39) | copy-start | bytes 6291460
Sparse Core Ops, SparseCore 0:
  16.7 63.6 all-gather.19
  83.2 111.0 all-gather.17
  261.2 6.0 reduce-scatter.2
  270.0 142.5 all-gather.11
  415.1 139.5 all-gather.13
  557.3 180.2 all-gather.15
  750.2 6.0 reduce-scatter.4
where the time goes:
time: 768 us; the launch traced here: 765 us
  waiting for transfers between devices  564 us (73%)
  other arithmetic  79.1 us (10%)
  blocking collectives  46.5 us (6%)
  matrix products  35.6 us (5%)
  local copies, waits for them, and re-layouts  24.3 us (3%)
  between operations  14.5 us (2%)
    all_gather x1, waiting for transfers between devices, body(): lax.all_gather(down_weight, 'sp', axis=1, tiled=True)  183 us
    all_gather x1, waiting for transfers between devices, body(): lax.all_gather(gate_weight, 'sp', axis=0, tiled=True)  141 us
    all_gather x1, waiting for transfers between devices, body(): lax.all_gather(up_weight, 'sp', axis=0, tiled=True)  135 us
    all_gather x2, waiting for transfers between devices, entering(): everything = jax.tree.map(lambda part: lax.all_gather(part, axis), value)  93 us
    select_n x48, other arithmetic, step(): return jax.tree.map(lambda a, b: jnp.where(reached, a, b), new, before)  55.7 us
    unnamed x1, blocking collectives  44.1 us
  transfers between devices with their start and end apart: 7, of which 6 were waited for; matrix products, arithmetic and copies ran while one was open for 6% of the time, Pallas kernels for 0%

commit v1 on v0

v1 whole, which is shorter than its diff:
```python
import functools

import jax
import jax.numpy as jnp
from jax import lax
from jax.experimental import pallas as pl
from jax.experimental.pallas import tpu as pltpu
from jax.sharding import Mesh, PartitionSpec as P

DK_A = 128
DK_B = 64
LOW = -1e30
MESH = pl.DeviceIdType.MESH


def cell_kernel(
    n,
    q_w,
    k_w,
    v_w,
    og_w,
    gain_w,
    q_n,
    k_n,
    v_n,
    og_n,
    gain_n,
    gating,
    out_w,
    out_n,
    raw_w,
    raw_n,
    stabs,
    sent,
    got,
    back,
    carried,
    mem_w,
    mem_n,
    state,
    levels,
    send_sem,
    recv_sem,
    send_sem2,
    recv_sem2,
):
    na, nb = lax.axis_size("a"), lax.axis_size("b")
    tp = lax.axis_index("tp")
    me = lax.axis_index("a") * nb + lax.axis_index("b")

    def where_is(index):
        return (index // nb, lax.rem(index, nb), tp)

    barrier = pltpu.get_barrier_semaphore()

    def greet(r, _):
        peer = lax.rem(me + r, n)
        pl.semaphore_signal(barrier, inc=1, device_id=where_is(peer), device_id_type=MESH)
        return 0

    lax.fori_loop(1, n, greet, 0)

    rows = q_w.shape[0]
    heads_p = gating.shape[1]
    groups = (
        (q_w, k_w, v_w, og_w, gain_w, out_w, raw_w, mem_w, DK_A),
        (q_n, k_n, v_n, og_n, gain_n, out_n, raw_n, mem_n, DK_B),
    )
    heads = tuple(g[0].shape[1] // g[8] for g in groups)
    parts = tuple(h * g[8] // n for h, g in zip(heads, groups))
    starts = (0, parts[0])
    extra = parts[0] + parts[1]

    it = lax.broadcasted_iota(jnp.int32, (rows, rows), 0)
    js = lax.broadcasted_iota(jnp.int32, (rows, rows), 1)
    upper = (it <= js).astype(jnp.float32)
    eye = (it == js).astype(jnp.float32)
    last_dims = (((1,), (1,)), ((), ()))
    first_dims = (((0,), (0,)), ((), ()))
    gate_in = gating[0]
    x = gating[1]
    forget = jnp.minimum(x, 0.0) - jnp.log1p(jnp.exp(-jnp.abs(x))) + gating[2]
    cum = jnp.dot(
        forget, upper, precision=lax.Precision.HIGHEST, preferred_element_type=jnp.float32
    )
    cum_t = lax.dot_general(
        eye, cum, last_dims, precision=lax.Precision.HIGHEST, preferred_element_type=jnp.float32
    )
    diff = gate_in - cum
    diff_t = lax.dot_general(
        eye, diff, last_dims, precision=lax.Precision.HIGHEST, preferred_element_type=jnp.float32
    )
    total = cum[:, rows - 1 : rows]
    level = jnp.max(total + diff, axis=1, keepdims=True)
    total_t = cum_t[rows - 1 : rows, :]
    level_t = jnp.max(total_t + diff_t, axis=0, keepdims=True)
    tail_t = jnp.exp(total_t + diff_t - level_t)
    width = sent.shape[2]
    lane = lax.broadcasted_iota(jnp.int32, (heads_p, width), 1)
    marks = jnp.where(
        lane < width // 2,
        jnp.broadcast_to(level, (heads_p, width)),
        jnp.broadcast_to(total, (heads_p, width)),
    )

    index = 0
    for g, (q, k, v, _, _, _, raw, _, dk) in enumerate(groups):
        dv = v.shape[1] // heads[g]
        scale = dk ** (-0.5)
        for h in range(heads[g]):
            k_h = k[:, h * dk : (h + 1) * dk]
            v_h = v[:, h * dv : (h + 1) * dv]
            scaled = k_h.astype(jnp.float32) * (tail_t[:, index : index + 1] * scale)
            memory = lax.dot_general(
                scaled.astype(jnp.bfloat16), v_h, first_dims, preferred_element_type=jnp.float32
            )
            size = parts[g]
            per = dk // size
            for p in range(per):
                sent[h * per + p, starts[g] : starts[g] + size, :dv] = memory[
                    p * size : (p + 1) * size
                ]
            index += 1
    spare = v_n.shape[1] // heads[1]
    if spare < width:
        sent[:, starts[1] : extra, spare:] = jnp.zeros((n, parts[1], width - spare), jnp.float32)
    for p in range(n):
        sent[p, extra : extra + heads_p, :] = marks

    pl.semaphore_wait(barrier, n - 1)

    def out_copy(r):
        peer = lax.rem(me + r, n)
        return pltpu.make_async_remote_copy(
            src_ref=sent.at[peer],
            dst_ref=got.at[me],
            send_sem=send_sem.at[r],
            recv_sem=recv_sem.at[r],
            device_id=where_is(peer),
            device_id_type=MESH,
        )

    lax.fori_loop(1, n, lambda r, c: (out_copy(r).start(), c)[1], 0)
    got[me] = sent[me]

    index = 0
    for g, (q, k, v, _, _, _, raw, _, dk) in enumerate(groups):
        dv = v.shape[1] // heads[g]
        scale = dk ** (-0.5)
        for h in range(heads[g]):
            q_h = q[:, h * dk : (h + 1) * dk]
            k_h = k[:, h * dk : (h + 1) * dk]
            v_h = v[:, h * dv : (h + 1) * dv]
            scores = lax.dot_general(q_h, k_h, last_dims, preferred_element_type=jnp.float32)
            logits = cum_t[:, index : index + 1] + diff[index : index + 1, :]
            logits = jnp.where(js <= it, logits, LOW)
            stab = jnp.max(logits, axis=1, keepdims=True)
            weighted = scores * scale * jnp.exp(logits - stab)
            raw[:, h * dv : (h + 1) * dv] = jnp.dot(
                weighted.astype(jnp.bfloat16), v_h, preferred_element_type=jnp.float32
            )
            stabs[:, index : index + 1] = stab
            index += 1

    lax.fori_loop(1, n, lambda r, c: (out_copy(r).wait(), c)[1], 0)

    which = tuple(
        (me * parts[g]) // groups[g][8] + (heads[0] if g else 0) for g in range(2)
    )
    sub = lax.broadcasted_iota(jnp.int32, (heads_p, width), 0)
    picks = tuple(sub == w for w in which)

    def merge(t, _):
        level_c = levels[0]
        back[t] = state[...]
        levels[1] = jnp.where(t == me, level_c, levels[1])
        mark = got[t, extra : extra + heads_p, :]
        lev = jnp.broadcast_to(mark[:, :1], mark.shape)
        tot = jnp.broadcast_to(mark[:, width - 1 :], mark.shape)
        new = jnp.maximum(level_c + tot, lev)
        old_f = jnp.exp(level_c + tot - new)
        new_f = jnp.exp(lev - new)
        levels[0] = new
        for g in range(2):
            span = slice(starts[g], starts[g] + parts[g])

            def pick(f):
                return jnp.sum(jnp.where(picks[g], f, 0.0), axis=0, keepdims=True)

            state[span, :] = pick(old_f) * state[span, :] + pick(new_f) * got[t, span, :]
        return 0

    levels[...] = jnp.full(levels.shape, LOW, jnp.float32)
    state[...] = jnp.zeros(state.shape, jnp.float32)
    lax.fori_loop(0, n, merge, 0)
    entering = levels[1]

    def back_copy(r):
        peer = lax.rem(me + r, n)
        return pltpu.make_async_remote_copy(
            src_ref=back.at[peer],
            dst_ref=carried.at[me],
            send_sem=send_sem2.at[r],
            recv_sem=recv_sem2.at[r],
            device_id=where_is(peer),
            device_id_type=MESH,
        )

    lax.fori_loop(1, n, lambda r, c: (back_copy(r).start(), c)[1], 0)
    carried[me] = back[me]
    entering_t = lax.dot_general(
        jnp.where(
            lax.broadcasted_iota(jnp.int32, (rows, width), 1) == 0, 1.0, 0.0
        ),
        entering,
        last_dims,
        precision=lax.Precision.HIGHEST,
        preferred_element_type=jnp.float32,
    )
    shifted = cum_t + entering_t
    own = stabs[:, :heads_p]
    both = jnp.maximum(own, shifted)
    own_f = jnp.exp(own - both)
    in_f = jnp.exp(shifted - both)
    lax.fori_loop(1, n, lambda r, c: (back_copy(r).wait(), c)[1], 0)

    index = 0
    for g, (q, _, v, og, gain, out, raw, mem, dk) in enumerate(groups):
        dv = v.shape[1] // heads[g]
        size = parts[g]
        per = dk // size
        for h in range(heads[g]):
            for p in range(per):
                mem[p * size : (p + 1) * size, :] = carried[
                    h * per + p, starts[g] : starts[g] + size, :dv
                ]
            memory = mem[...]
            high = memory.astype(jnp.bfloat16)
            rest = (memory - high.astype(jnp.float32)).astype(jnp.bfloat16)
            q_h = q[:, h * dk : (h + 1) * dk]
            cols = slice(h * dv, (h + 1) * dv)
            incoming = jnp.dot(q_h, high, preferred_element_type=jnp.float32) + jnp.dot(
                q_h, rest, preferred_element_type=jnp.float32
            )
            value = (
                raw[:, cols] * own_f[:, index : index + 1]
                + incoming * in_f[:, index : index + 1]
            )
            value = value * lax.rsqrt(jnp.mean(value * value, axis=1, keepdims=True) + 1e-06)
            gate = 1.0 / (1.0 + jnp.exp(-og[:, cols].astype(jnp.float32)))
            value = value * gain[:, cols].astype(jnp.float32) * gate
            out[:, cols] = value.astype(jnp.bfloat16)
            index += 1


def cell(q_w, k_w, v_w, og_w, gat_w, gain_w, q_n, k_n, v_n, og_n, gat_n, gain_n):
    n = lax.axis_size("a") * lax.axis_size("b")
    rows = q_w.shape[0]
    heads = gat_w.shape[1] + gat_n.shape[1]
    heads_p = -(-heads // 8) * 8
    gating = jnp.concatenate([gat_w, gat_n], axis=1)
    gating = jnp.pad(gating, ((0, 0), (0, heads_p - heads), (0, 0)))
    parts = (q_w.shape[1] // n, q_n.shape[1] // n)
    width = v_w.shape[1] // gat_w.shape[1]
    width_n = v_n.shape[1] // gat_n.shape[1]
    vmem = pl.BlockSpec(memory_space=pltpu.VMEM)
    state = parts[0] + parts[1]
    return pl.pallas_call(
        functools.partial(cell_kernel, n),
        out_shape=(
            jax.ShapeDtypeStruct(v_w.shape, jnp.bfloat16),
            jax.ShapeDtypeStruct(v_n.shape, jnp.bfloat16),
        ),
        in_specs=[vmem] * 11,
        out_specs=(vmem, vmem),
        scratch_shapes=[
            pltpu.VMEM(v_w.shape, jnp.float32),
            pltpu.VMEM(v_n.shape, jnp.float32),
            pltpu.VMEM((rows, 128), jnp.float32),
            pltpu.VMEM((n, state + heads_p, width), jnp.float32),
            pltpu.VMEM((n, state + heads_p, width), jnp.float32),
            pltpu.VMEM((n, state, width), jnp.float32),
            pltpu.VMEM((n, state, width), jnp.float32),
            pltpu.VMEM((DK_A, width), jnp.float32),
            pltpu.VMEM((DK_B, width_n), jnp.float32),
            pltpu.VMEM((state, width), jnp.float32),
            pltpu.VMEM((2, heads_p, width), jnp.float32),
            pltpu.SemaphoreType.DMA((n,)),
            pltpu.SemaphoreType.DMA((n,)),
            pltpu.SemaphoreType.DMA((n,)),
            pltpu.SemaphoreType.DMA((n,)),
        ],
        compiler_params=pltpu.CompilerParams(
            collective_id=0, has_side_effects=True, vmem_limit_bytes=32 * 2**20
        ),
        cost_estimate=pl.CostEstimate(
            flops=2 * 10**9, bytes_accessed=120 * 10**6, transcendentals=0
        ),
    )(
        q_w,
        k_w,
        v_w,
        og_w,
        gain_w.reshape(1, -1),
        q_n,
        k_n,
        v_n,
        og_n,
        gain_n.reshape(1, -1),
        gating,
    )


def body(
    residual,
    query_wide,
    key_wide,
    value_wide,
    outgate_wide,
    gating_wide,
    gain_wide,
    readout_wide,
    query_narrow,
    key_narrow,
    value_narrow,
    outgate_narrow,
    gating_narrow,
    gain_narrow,
    readout_narrow,
    norm_gain,
    gate_weight,
    up_weight,
    down_weight,
):
    na, nb = lax.axis_size("a"), lax.axis_size("b")
    depth, hidden_tp = gate_weight.shape
    chunk = hidden_tp // na
    out_cols = down_weight.shape[1]
    model = residual.shape[1]

    def regroup(pieces):
        mine = lax.all_to_all(pieces, "a", split_axis=0, concat_axis=0, tiled=True)
        return lax.all_gather(mine, "b", axis=0, tiled=True)

    gate_all = regroup(jnp.moveaxis(gate_weight.reshape(depth, na, chunk), 1, 0))
    up_all = regroup(jnp.moveaxis(up_weight.reshape(depth, na, chunk), 1, 0))
    down_all = regroup(down_weight.reshape(na, chunk, out_cols))

    gated_w, gated_n = cell(
        query_wide,
        key_wide,
        value_wide,
        outgate_wide,
        gating_wide,
        gain_wide,
        query_narrow,
        key_narrow,
        value_narrow,
        outgate_narrow,
        gating_narrow,
        gain_narrow,
    )
    mixed = lax.psum_scatter(
        (
            jnp.dot(gated_w, readout_wide, preferred_element_type=jnp.float32)
            + jnp.dot(gated_n, readout_narrow, preferred_element_type=jnp.float32)
        ).astype(jnp.bfloat16),
        "tp",
        scatter_dimension=0,
        tiled=True,
    ).astype(jnp.float32)
    middle_f = (residual.astype(jnp.float32) + mixed).astype(jnp.bfloat16).astype(jnp.float32)
    normed = middle_f * lax.rsqrt(jnp.mean(middle_f * middle_f, axis=-1, keepdims=True) + 1e-06)
    normed = (normed * norm_gain.astype(jnp.float32)).astype(jnp.bfloat16)
    own_rows = normed.shape[0]
    normed = normed.reshape(own_rows, na, nb, depth).swapaxes(1, 2).reshape(own_rows, model)
    all_rows = lax.all_gather(normed, ("a", "tp"), axis=0, tiled=True)
    gate = jnp.dot(all_rows, gate_all.reshape(model, chunk), preferred_element_type=jnp.float32)
    upper = jnp.dot(all_rows, up_all.reshape(model, chunk), preferred_element_type=jnp.float32)
    hidden = (jax.nn.silu(gate) * upper).astype(jnp.bfloat16)
    down = jnp.transpose(down_all, (1, 0, 2)).reshape(chunk, model)
    terms = jnp.dot(hidden, down, preferred_element_type=jnp.float32)
    back = lax.psum_scatter(
        terms.astype(jnp.bfloat16), ("a", "tp"), scatter_dimension=0, tiled=True
    ).astype(jnp.float32)
    back = back.reshape(own_rows, nb, na, out_cols).swapaxes(1, 2).reshape(own_rows, model)
    return (middle_f + back).astype(jnp.bfloat16)


def solution(mesh):
    sp, tp = mesh.shape["sp"], mesh.shape["tp"]
    a = 4 if sp % 4 == 0 else 1
    split = Mesh(mesh.devices.reshape(a, sp // a, tp), ("a", "b", "tp"))
    s = ("a", "b")
    in_specs = (
        P(("a", "b", "tp"), None),
        P(s, "tp"),
        P(s, "tp"),
        P(s, "tp"),
        P(s, "tp"),
        P(None, "tp", s),
        P("tp"),
        P("tp", None),
        P(s, "tp"),
        P(s, "tp"),
        P(s, "tp"),
        P(s, "tp"),
        P(None, "tp", s),
        P("tp"),
        P("tp", None),
        P(),
        P(s, "tp"),
        P(s, "tp"),
        P("tp", s),
    )
    out_specs = P(("a", "b", "tp"), None)
    return jax.shard_map(body, mesh=split, in_specs=in_specs, out_specs=out_specs, check_vma=False)
```

time: 768 us -> 309 us (0.40)
  waiting for transfers between devices: 564 us -> 132 us
  other arithmetic: 79.1 us -> 3.72 us
  Pallas kernels: 0 us -> 44.9 us
  blocking collectives: 46.5 us -> 81.5 us
  matrix products: 35.6 us -> 15.7 us
  local copies, waits for them, and re-layouts: 24.3 us -> 16.4 us
    all_gather x5 -> x4, waiting for transfers between devices: 552 us -> 83.1 us  [the longest x3 83.1 us: regroup(): return lax.all_gather(mine, 'b', axis=0, tiled=True)]
    all_to_all x0 -> x3, blocking collectives: none -> 81.5 us  [regroup(): mine = lax.all_to_all(pieces, 'a', split_axis=0, concat_axis=0, tiled=True)]
    select_n x48 -> x0, other arithmetic: 55.7 us -> none  [step(): return jax.tree.map(lambda a, b: jnp.where(reached, a, b), new, before)]
    pallas_call x0 -> x1, Pallas kernels: none -> 44.9 us  [cell(): pl.pallas_call(functools.partial(cell_kernel, n), out_shape=(jax.ShapeDty...]
    unnamed x1 -> x0, blocking collectives: 44.1 us -> none
    reduce_scatter x1, waiting for transfers between devices: 6.26 us -> 36.2 us  [body(): lax.psum_scatter(terms.astype(jnp.bfloat16), ('a', 'tp'), scatter_dimensi...]
    dot_general x16 -> x2, matrix products: 31.3 us -> 13.7 us  [the longest x1 8.5 us: body(): terms = jnp.dot(hidden, down, preferred_element_type=jnp.float32)]
    reduce_scatter x1, waiting for transfers between devices: 4.45 us -> 12.6 us  [body(): lax.psum_scatter((jnp.dot(gated_w, readout_wide, preferred_element_type=j...]
  transfers between devices with their start and end apart: 7 -> 6, of which waited for: 6 -> 5; matrix products, arithmetic and copies ran while one was open for 6% -> 3% of each run, Pallas kernels for 0% -> 0%
where the time goes in v1:
time: 309 us; the launch traced here: 308 us
  waiting for transfers between devices  132 us (43%)
  blocking collectives  81.5 us (26%)
  Pallas kernels  44.9 us (15%)
  local copies, waits for them, and re-layouts  16.4 us (5%)
  matrix products  15.7 us (5%)
  between operations  13.6 us (4%)
  other arithmetic  3.72 us (1%)
    all_gather x3, waiting for transfers between devices, regroup(): return lax.all_gather(mine, 'b', axis=0, tiled=True)  83.1 us
    all_to_all x3, blocking collectives, regroup(): mine = lax.all_to_all(pieces, 'a', split_axis=0, concat_axis=0, tiled=True)  81.5 us
    pallas_call x1, Pallas kernels, cell(): pl.pallas_call(functools.partial(cell_kernel, n), out_shape=(jax.ShapeDty...  44.9 us
    reduce_scatter x1, waiting for transfers between devices, body(): lax.psum_scatter(terms.astype(jnp.bfloat16), ('a', 'tp'), scatter_dimensi...  36.2 us
    reduce_scatter x1, waiting for transfers between devices, body(): lax.psum_scatter((jnp.dot(gated_w, readout_wide, preferred_element_type=j...  12.6 us
    unnamed x28, local copies, waits for them, and re-layouts  10.1 us
    dot_general x1, matrix products, body(): terms = jnp.dot(hidden, down, preferred_element_type=jnp.float32)  8.5 us
  transfers between devices with their start and end apart: 6, of which 5 were waited for; matrix products, arithmetic and copies ran while one was open for 3% of the time, Pallas kernels for 0%

profile of v1, /device:TPU:0, one launch (start us, length us, event | category | flops | bytes accessed | tf_op | source)
XLA Modules:
  0.0 308.1 jit_solution(11888291654789052531)
XLA Ops:
  6.5 0.8 reshape.49.gain_w
  7.4 0.7 reshape.50.gain_n
  8.1 0.7 pad_maximum_fusion.gating
  8.8 0.9 copy-done.1
  9.7 0.9 copy-done.2
  10.7 0.9 copy-done.3
  11.6 0.9 copy-done.4
  12.5 0.9 copy-done.5
  13.4 0.9 copy-done.6
  14.3 0.8 copy-done.7
  15.1 0.8 copy-done.8
  16.0 44.9 %shard_map.181 = (bf16[128,1024]{1,0:T(8,128)(2,1)S(1)}, bf16[128,512]{1,0:T(8,128)(2,1)S(1)}) custom-call(bf16[128,512]{1,0:T(8,128)(2,1)S(1)} %copy-done.3, bf16[128,512]{1,0:T(8,128)(2,1)S(1)} %copy-done.4, bf16[128,1024]{1,0:T(8,128)(2,1)S(1)} %copy-done.1, bf16[128,1024]{1,0:T(8,128)(2,1)S(1)} %copy-done.2, bf16[1,1024]{1,0:T(2,128)(2,1)S(1)} %reshape.49.gain_w, ...), custom_call_target="tpu_custom_call" | custom-call | flops 2000000000 | bytes 120000000 | tf_op jit(solution)/shard_map/pallas_call | solution.py:268
  60.9 0.7 fusion.23
  61.7 0.0 copy-start.10
  61.7 1.3 fusion.8
  63.0 0.0 reduce-scatter.3.cloned.1.call-update
  63.0 0.0 all-gather.5.cloned.1.call-start
  63.1 12.6 %reduce-scatter.3.cloned.1.call-done = bf16[64,2048]{1,0:T(8,128)(2,1)} async-done(((bf16[128,2048]{1,0:T(8,128)(2,1)}), bf16[64,2048]{1,0:T(8,128)(2,1)}) %reduce-scatter.3.cloned.1.call-update) | async-done | bytes 262160 | tf_op jit(solution)/shard_map/reduce_scatter | solution.py:363
  75.7 1.1 fusion.18
  76.8 1.1 fusion.20
  77.9 0.2 reshape.51
  78.1 0.1 copy.59
  78.2 0.9 reshape.52
  79.1 0.0 all-gather.5.cloned.1.call-update
  79.1 0.0 all-gather.7.cloned.1.call-start
  79.1 1.5 copy.29
  80.6 39.6 %all_to_all.15 = bf16[4,128,704]{1,2,0:T(8,128)(2,1)} all-to-all(bf16[4,128,704]{1,2,0:T(8,128)(2,1)S(1)} %bitcast.48), channel_id=1, replica_groups=mesh['a'=4,'b'=4,'tp'=2] {'a'}, dimensions={0} | all-to-all | bytes 1441792 | tf_op jit(solution)/shard_map/all_to_all | solution.py:342
  120.2 0.0 all-gather.7.cloned.1.call-update
  120.3 0.0 all-gather.9.cloned.1.call-start
  120.3 1.5 copy.31
  121.8 20.2 %all_to_all.16 = bf16[4,128,704]{1,2,0:T(8,128)(2,1)} all-to-all(bf16[4,128,704]{1,2,0:T(8,128)(2,1)S(1)} %bitcast.49), channel_id=1, replica_groups=mesh['a'=4,'b'=4,'tp'=2] {'a'}, dimensions={0} | all-to-all | bytes 1441792 | tf_op jit(solution)/shard_map/all_to_all | solution.py:342
  142.0 0.0 all-gather.9.cloned.1.call-update
  142.0 0.0 all-gather.11.cloned.1.call-start
  142.1 21.6 %all_to_all.17 = bf16[4,704,128]{2,1,0:T(8,128)(2,1)} all-to-all(bf16[4,704,128]{2,1,0:T(8,128)(2,1)} %bitcast.52), channel_id=1, replica_groups=mesh['a'=4,'b'=4,'tp'=2] {'a'}, dimensions={0} | all-to-all | bytes 1441792 | tf_op jit(solution)/shard_map/all_to_all | solution.py:342
  163.7 0.0 all-gather.11.cloned.1.call-update
  163.7 0.0 reduce-scatter.5.cloned.1.call-start
  163.8 0.0 all-gather.5.cloned.1.call-done
  163.8 1.6 all-gather.7.cloned.1.call-done
  165.4 5.2 %fusion.5 = f32[512,704]{0,1:T(8,128)} fusion(bf16[512,2048]{1,0:T(8,128)(2,1)} %all-gather.5.cloned.1.call-done, bf16[16,128,704]{1,2,0:T(8,128)(2,1)} %all-gather.7.cloned.1.call-done), kind=kOutput, calls=%fused_computation.6 | convolution fusion | flops 1476395008 | bytes 6422528 | tf_op jit(solution)/shard_map/dot_general | solution.py:378
  170.6 38.2 %all-gather.9.cloned.1.call-done = bf16[16,128,704]{1,2,0:T(8,128)(2,1)} async-done(((bf16[4,128,704]{1,2,0:T(8,128)(2,1)}), bf16[16,128,704]{1,2,0:T(8,128)(2,1)}) %all-gather.9.cloned.1.call-update) | async-done | bytes 2883600 | tf_op jit(solution)/shard_map/all_gather | solution.py:343
  208.8 43.4 %all-gather.11.cloned.1.call-done = bf16[16,704,128]{2,1,0:T(8,128)(2,1)} async-done(((bf16[4,704,128]{2,1,0:T(8,128)(2,1)}), bf16[16,704,128]{2,1,0:T(8,128)(2,1)}) %all-gather.11.cloned.1.call-update) | async-done | bytes 2883600 | tf_op jit(solution)/shard_map/all_gather | solution.py:343
  252.2 8.5 %convolution_convert_fusion = bf16[512,2048]{1,0:T(8,128)(2,1)} fusion(bf16[512,2048]{1,0:T(8,128)(2,1)} %all-gather.5.cloned.1.call-done, f32[512,704]{0,1:T(8,128)} %fusion.5, bf16[16,704,128]{2,1,0:T(8,128)(2,1)} %all-gather.11.cloned.1.call-done, bf16[16,128,704]{1,2,0:T(8,128)(2,1)} %all-gather.9.cloned.1.call-done), kind=kOutput, calls=%fused_computation | convolution fusion | flops 2956001280 | bytes 11403264 | tf_op jit(solution)/shard_map/dot_general | solution.py:382
  260.7 0.0 reduce-scatter.5.cloned.1.call-update
  260.7 36.2 %reduce-scatter.5.cloned.1.call-done = bf16[64,2048]{1,0:T(8,128)(2,1)} async-done(((bf16[512,2048]{1,0:T(8,128)(2,1)}), bf16[64,2048]{1,0:T(8,128)(2,1)}) %reduce-scatter.5.cloned.1.call-update) | async-done | bytes 262160 | tf_op jit(solution)/shard_map/reduce_scatter | solution.py:383
  296.9 1.4 reshape.66
  298.3 0.9 copy.58
  299.2 1.3 reshape.63
  300.5 0.8 fusion.21
  (20 shorter events, 0.0 us)
Async XLA Ops:
  6.5 55.1 %copy-start = (bf16[512,2048]{1,0:T(8,128)(2,1)S(1)}, bf16[512,2048]{1,0:T(8,128)(2,1)}, u32[]{:S(2)}) copy-start(bf16[512,2048]{1,0:T(8,128)(2,1)} %param.33) | copy-start | bytes 6291460
  6.5 69.1 %reduce-scatter.3.cloned.1.call-start = ((), (), s32[]{:S(2)}) async-start(), calls=%async_computation.5 | async-start | bytes 786432 | tf_op jit(solution)/shard_map/reduce_scatter | solution.py:363
  8.8 0.9 copy-start.1
  9.7 0.9 copy-start.2
  10.7 0.9 copy-start.3
  11.6 0.9 copy-start.4
  12.5 0.9 copy-start.5
  13.4 0.9 copy-start.6
  14.3 0.8 copy-start.7
  15.1 0.8 copy-start.8
  16.0 44.9 %copy-start.9 = (bf16[1024,2048]{1,0:T(8,128)(2,1)S(1)}, bf16[1024,2048]{1,0:T(8,128)(2,1)}, u32[]{:S(2)}) copy-start(bf16[1024,2048]{1,0:T(8,128)(2,1)} %param.26) | copy-start | bytes 12582916
  61.6 1.4 copy-start.12
  61.7 14.0 %copy-start.10 = (bf16[64,2048]{1,0:T(8,128)(2,1)S(1)}, bf16[64,2048]{1,0:T(8,128)(2,1)}, u32[]{:S(2)}) copy-start(bf16[64,2048]{1,0:T(8,128)(2,1)} %param.19) | copy-start | bytes 786436
  63.0 100.8 %all-gather.5.cloned.1.call-start = ((), (), s32[]{:S(2)}) async-start(), calls=%async_computation.6 | async-start | bytes 2359296 | tf_op jit(solution)/shard_map/all_gather | solution.py:377
  79.1 86.3 %all-gather.7.cloned.1.call-start = ((), (), s32[]{:S(2)}) async-start(), calls=%async_computation.7 | async-start | bytes 3604480 | tf_op jit(solution)/shard_map/all_gather | solution.py:343
  120.3 88.5 %all-gather.9.cloned.1.call-start = ((), (), s32[]{:S(2)}) async-start(), calls=%async_computation.8 | async-start | bytes 3604480 | tf_op jit(solution)/shard_map/all_gather | solution.py:343
  142.0 110.1 %all-gather.11.cloned.1.call-start = ((), (), s32[]{:S(2)}) async-start(), calls=%async_computation.9 | async-start | bytes 3604480 | tf_op jit(solution)/shard_map/all_gather | solution.py:343
  163.7 133.2 %reduce-scatter.5.cloned.1.call-start = ((), (), s32[]{:S(2)}) async-start(), calls=%async_computation.10 | async-start | bytes 2359296 | tf_op jit(solution)/shard_map/reduce_scatter | solution.py:383
  260.7 39.8 %copy-start.11 = (bf16[64,2048]{1,0:T(8,128)(2,1)S(1)}, bf16[64,2048]{1,0:T(8,128)(2,1)}, u32[]{:S(2)}) copy-start(bf16[64,2048]{1,0:T(8,128)(2,1)} %reduce-scatter.3.cloned.1.call-done) | copy-start | bytes 786436
Sparse Core Ops, SparseCore 0:
  63.1 12.5 reduce-scatter.2
  79.2 43.5 all-gather.4
  124.6 40.6 all-gather.6
  167.1 41.6 all-gather.8
  210.5 41.6 all-gather.10
  260.8 36.0 reduce-scatter.4
